TPU v7x, 32 devices: a whole 2x2x4 slice. The times are simulated.
32 devices in a mesh: ep: 16 (over z, x, core), tp: 2 (over y).
Axes of the slice: x: 2, y: 2, z: 4, core: 2. Of those that a mesh axis runs over, the one named last changes fastest.
Arguments:
- hidden_in: bfloat16 [256, 1024], P('ep', 'tp'), may hold values from -40 to 40
- norm_gain_attn: float32 [1024], replicated, may hold values from 0.1 to 1.9
- query_weight: bfloat16 [1024, 512], P(None, 'tp'), may hold values from -0.1875 to 0.1875
- key_weight: bfloat16 [1024, 512], P(None, 'tp'), may hold values from -0.1875 to 0.1875
- value_weight: bfloat16 [1024, 512], P(None, 'tp'), may hold values from -0.1875 to 0.1875
- query_gain: float32 [128], replicated, may hold values from 1 to 1.6
- key_gain: float32 [128], replicated, may hold values from 1 to 1.6
- lambda_head: float32 [4], P('tp'), may hold values from 0.3 to 0.8
- sub_gain: float32 [128], replicated, may hold values from 0.1 to 1.9
- out_weight: bfloat16 [512, 1024], P('tp'), may hold values from -0.25 to 0.25
- cache_key: bfloat16 [256, 256, 512], P('ep', None, 'tp'), may hold values from -8 to 8
- cache_value: bfloat16 [256, 256, 512], P('ep', None, 'tp'), may hold values from -6 to 6
- lengths: int32 [256], P('ep'), may hold values from 1 to 256
- norm_gain_mix: float32 [1024], P('tp'), may hold values from 0.1 to 1.9
- route_ids: int32 [256, 6], P('ep'), may hold values from 0 to 15, all different within a row; in each aligned block of 16 rows (0 to 15, 16 to 31, ...) at most 12 rows name the same one
- route_logits: float32 [256, 6], P('ep'), may hold values from -4 to 4
- expert_gate: bfloat16 [16, 1024, 1024], P('ep', None, 'tp'), may hold values from -0.5 to 0.5
- expert_up: bfloat16 [16, 1024, 1024], P('ep', None, 'tp'), may hold values from -0.5 to 0.5
- expert_down: bfloat16 [16, 1024, 1024], P('ep', 'tp'), may hold values from -0.046875 to 0.046875
- dense_gate: bfloat16 [1024, 2048], P('tp', 'ep'), may hold values from -0.1875 to 0.1875
- dense_up: bfloat16 [1024, 2048], P('tp', 'ep'), may hold values from -0.1875 to 0.1875
- dense_down: bfloat16 [2048, 1024], P('ep', 'tp'), may hold values from -0.125 to 0.125
- branch_gate: float32 [1024], P('tp'), may hold values from -0.1875 to 0.1875
Outputs:
- layer_out: bfloat16 [256, 1024], P('ep', 'tp')
- key_rows: bfloat16 [256, 512], P('ep', 'tp')
- value_rows: bfloat16 [256, 512], P('ep', 'tp')
Inputs may be any that keep to these rules, and one draw needn't show every extreme that they name: `route_ids`: each row names 6 different experts. Among the rows of one index of ep (aligned blocks of 16 rows) no expert is named by more than 12 rows, and in some blocks one expert is named by exactly 12.
All inputs are finite; a program needn't handle non-finite values.
Results may differ from a plain program's by a relative error of at most 0.0075.
Values may be sent and summed in bfloat16 or wider, within the bound.
A program may use at most 64 MiB of HBM per device.

v0:
```python
import math

import jax
import jax.numpy as jnp
from jax import lax
from jax.sharding import PartitionSpec as P

EPSILON = 1e-06
CLAMP_LIMIT = 7.0
SWISH_ALPHA = 1.702
OUT_SCALE = 0.2 + 0.6 * math.exp(-0.6)


def rms_scale(values, scale_gain):
    mean_square = jnp.mean(values * values, axis=-1, keepdims=True)
    return values * lax.rsqrt(mean_square + EPSILON) * scale_gain


def clamped_unit(gate_pre, up_pre):
    gate_cut = jnp.minimum(gate_pre, CLAMP_LIMIT)
    up_cut = jnp.clip(up_pre, -CLAMP_LIMIT, CLAMP_LIMIT)
    return (up_cut + 1.0) * gate_cut * jax.nn.sigmoid(SWISH_ALPHA * gate_cut)


def attend(
    normed,
    query_weight,
    key_weight,
    value_weight,
    query_gain,
    key_gain,
    lambda_head,
    sub_gain,
    cache_key,
    cache_value,
    lengths,
):
    seq_count = normed.shape[0]
    head_count = lambda_head.shape[0]
    qk_size = query_gain.shape[0] // 2
    val_size = value_weight.shape[1] // head_count
    cache_len = cache_key.shape[1]
    scale_factor = qk_size ** (-0.5)
    query_pre = jnp.dot(normed, query_weight, preferred_element_type=jnp.float32)
    query_rows = rms_scale(
        query_pre.reshape(seq_count, head_count, 2, qk_size), query_gain.reshape(2, qk_size)
    ).astype(jnp.bfloat16)
    key_pre = jnp.dot(normed, key_weight, preferred_element_type=jnp.float32)
    key_rows = rms_scale(
        key_pre.reshape(seq_count, head_count, 2, qk_size), key_gain.reshape(2, qk_size)
    ).astype(jnp.bfloat16)
    value_rows = jnp.dot(normed, value_weight, preferred_element_type=jnp.float32).astype(
        jnp.bfloat16
    )
    key_past = cache_key.reshape(seq_count, cache_len, head_count, 2, qk_size)
    past_score = (
        jnp.einsum("shmd,sjhmd->shmj", query_rows, key_past, preferred_element_type=jnp.float32)
        * scale_factor
    )
    own_score = (
        jnp.einsum("shmd,shmd->shm", query_rows, key_rows, preferred_element_type=jnp.float32)
        * scale_factor
    )
    valid_mask = lax.iota(jnp.int32, cache_len)[None, :] < lengths[:, None]
    past_exp = jnp.where(valid_mask[:, None, None, :], jnp.exp(past_score), 0.0)
    own_exp = jnp.exp(own_score)
    denominator = jnp.sum(past_exp, axis=-1) + own_exp
    past_prob = past_exp / denominator[..., None]
    own_prob = own_exp / denominator
    weight_past = (past_prob[:, :, 0] - lambda_head[None, :, None] * past_prob[:, :, 1]).astype(
        jnp.bfloat16
    )
    weight_own = (own_prob[:, :, 0] - lambda_head[None, :] * own_prob[:, :, 1]).astype(jnp.bfloat16)
    value_past = cache_value.reshape(seq_count, cache_len, head_count, val_size)
    head_mix = jnp.einsum(
        "shj,sjhe->she", weight_past, value_past, preferred_element_type=jnp.float32
    )
    own_value = value_rows.reshape(seq_count, head_count, val_size).astype(jnp.float32)
    head_mix = head_mix + weight_own.astype(jnp.float32)[..., None] * own_value
    head_out = (rms_scale(head_mix, sub_gain) * OUT_SCALE).astype(jnp.bfloat16)
    return (
        head_out.reshape(seq_count, head_count * val_size),
        key_rows.reshape(seq_count, -1),
        value_rows,
    )


def body(
    hidden_in,
    norm_gain_attn,
    query_weight,
    key_weight,
    value_weight,
    query_gain,
    key_gain,
    lambda_head,
    sub_gain,
    out_weight,
    cache_key,
    cache_value,
    lengths,
    norm_gain_mix,
    route_ids,
    route_logits,
    expert_gate,
    expert_up,
    expert_down,
    dense_gate,
    dense_up,
    dense_down,
    branch_gate,
):
    seq_count, top_count = route_ids.shape
    full_rows = lax.all_gather(hidden_in, "tp", axis=1, tiled=True)
    width_total = full_rows.shape[1]
    normed = rms_scale(full_rows.astype(jnp.float32), norm_gain_attn).astype(jnp.bfloat16)
    head_out, key_rows, value_rows = attend(
        normed,
        query_weight,
        key_weight,
        value_weight,
        query_gain,
        key_gain,
        lambda_head,
        sub_gain,
        cache_key,
        cache_value,
        lengths,
    )
    head_terms = jnp.dot(head_out, out_weight, preferred_element_type=jnp.float32)
    attn_part = lax.psum_scatter(head_terms, "tp", scatter_dimension=1, tiled=True)
    residual = hidden_in.astype(jnp.float32) + attn_part
    square_sum = lax.psum(jnp.sum(residual * residual, axis=1), "tp")
    inverse = lax.rsqrt(square_sum / width_total + EPSILON)
    mix_float = residual * inverse[:, None] * norm_gain_mix[None, :]
    gate_logit = lax.psum(jnp.sum(mix_float * branch_gate[None, :], axis=1), "tp")
    branch_weight = jax.nn.sigmoid(gate_logit)[:, None]
    mix_rows = mix_float.astype(jnp.bfloat16)
    route_weight = jax.nn.softmax(route_logits, axis=1)
    experts = lax.axis_size("ep") * expert_gate.shape[0]
    capacity = min(seq_count, 2 * ((seq_count * top_count + experts - 1) // experts))
    flat_ids = route_ids.reshape(-1)
    one_hot = (flat_ids[:, None] == lax.iota(jnp.int32, experts)[None, :]).astype(jnp.int32)
    route_rank = jnp.sum((jnp.cumsum(one_hot, axis=0) - one_hot) * one_hot, axis=1)
    slot_index = flat_ids * capacity + route_rank
    select_matrix = (
        lax.iota(jnp.int32, experts * capacity)[:, None] == slot_index[None, :]
    ).astype(jnp.bfloat16)
    route_rows = jnp.repeat(mix_rows, top_count, axis=0)
    placed = jnp.dot(select_matrix, route_rows, preferred_element_type=jnp.float32)
    arrived = lax.all_gather(
        lax.all_to_all(
            placed.astype(jnp.bfloat16).reshape(experts, capacity, mix_rows.shape[1]),
            "ep",
            split_axis=0,
            concat_axis=0,
            tiled=True,
        ),
        "tp",
        axis=2,
        tiled=True,
    )
    source_count, item_count, width_now = arrived.shape
    flat_rows = arrived.reshape(source_count * item_count, width_now)
    gate_pre = jnp.dot(flat_rows, expert_gate[0], preferred_element_type=jnp.float32)
    up_pre = jnp.dot(flat_rows, expert_up[0], preferred_element_type=jnp.float32)
    activation = clamped_unit(gate_pre, up_pre).astype(jnp.bfloat16)
    partial_out = jnp.dot(activation, expert_down[0], preferred_element_type=jnp.float32)
    partial_out = partial_out.reshape(source_count, item_count, width_now)
    summed = lax.psum_scatter(partial_out, "tp", scatter_dimension=2, tiled=True).astype(
        jnp.bfloat16
    )
    returned = lax.all_to_all(summed, "ep", split_axis=0, concat_axis=0, tiled=True)
    local_width = returned.shape[2]
    route_out = jnp.dot(
        select_matrix.T,
        returned.reshape(experts * capacity, local_width),
        preferred_element_type=jnp.float32,
    )
    routed = jnp.sum(
        route_out.reshape(seq_count, top_count, local_width) * route_weight[:, :, None], axis=1
    )
    dense_cols = dense_gate.shape[1]
    pair_weight = jnp.concatenate([dense_gate, dense_up], axis=1)
    partial_pre = jnp.dot(
        lax.all_gather(mix_rows, "ep", axis=0, tiled=True),
        pair_weight,
        preferred_element_type=jnp.float32,
    )
    dense_pre = lax.psum(partial_pre, "tp")
    all_act = (jax.nn.silu(dense_pre[:, :dense_cols]) * dense_pre[:, dense_cols:]).astype(
        jnp.bfloat16
    )
    dense_result = lax.psum_scatter(
        jnp.dot(all_act, dense_down, preferred_element_type=jnp.float32),
        "ep",
        scatter_dimension=0,
        tiled=True,
    )
    layer_out = (residual + routed + branch_weight * dense_result).astype(jnp.bfloat16)
    return (layer_out, key_rows, value_rows)


def solution(mesh):
    in_specs = (
        P("ep", "tp"),
        P(),
        P(None, "tp"),
        P(None, "tp"),
        P(None, "tp"),
        P(),
        P(),
        P("tp"),
        P(),
        P("tp", None),
        P("ep", None, "tp"),
        P("ep", None, "tp"),
        P("ep"),
        P("tp"),
        P("ep", None),
        P("ep", None),
        P("ep", None, "tp"),
        P("ep", None, "tp"),
        P("ep", "tp", None),
        P("tp", "ep"),
        P("tp", "ep"),
        P("ep", "tp"),
        P("tp"),
    )
    out_specs = (P("ep", "tp"), P("ep", "tp"), P("ep", "tp"))
    return jax.shard_map(body, mesh=mesh, in_specs=in_specs, out_specs=out_specs, check_vma=False)
```

profile of v0, /device:TPU:0, one launch (start us, length us, event | category | flops | bytes accessed | tf_op | source)
XLA Modules:
  0.0 187.4 jit_solution(8986353031277056286)
XLA Ops:
  7.2 0.9 mul.233
  8.1 0.7 mul.225
  9.6 5.6 %all_gather.9 = bf16[16,1024]{1,0:T(8,128)(2,1)S(1)} all-gather(bf16[16,512]{1,0:T(8,128)(2,1)} %param.23), channel_id=1, replica_groups=mesh['ep'=16,'tp'=2] {'tp'}, dimensions={1}, use_global_device_ids=true | all-gather | bytes 49152 | tf_op jit(solution)/shard_map/all_gather | solution.py:114
  15.3 1.3 convolution_convert_fusion.1
  17.2 1.3 fusion.51
  18.5 1.3 fusion.53
  21.0 3.9 %copy.65 = bf16[16,256,256]{1,2,0:T(8,128)(2,1)} copy(bf16[16,256,256]{2,1,0:T(8,128)(2,1)} %param.33) | data formatting | bytes 4194304 | tf_op args[10]
  24.9 2.0 %fusion.36 = f32[16,2,2,1,256]{4,3,2,1,0:T(1,128)S(1)} fusion(bf16[16,256,2,2,64]{1,4,3,2,0:T(8,128)(2,1)} %bitcast.67, bf16[16,2,2,64,1]{3,2,1,0,4:T(2,128)(2,1)S(1)} %bitcast.68), kind=kOutput, calls=%fused_computation.51 | convolution fusion | flops 2097152 | bytes 2170880 | tf_op jit(solution)/shard_map/shmd,sjhmd->shmj/dot_general | solution.py:57
  28.2 0.8 fusion.40
  29.6 11.3 %reduce-scatter.4.cloned.1.call-done = f32[16,512]{1,0:T(8,128)} async-done(((f32[16,1024]{1,0:T(8,128)}), f32[16,512]{1,0:T(8,128)}) %reduce-scatter.4.cloned.1.call-update) | async-done | bytes 32784 | tf_op jit(solution)/shard_map/reduce_scatter | solution.py:131
  40.9 0.9 multiply_reduce_fusion.1
  41.7 4.9 %psum.21 = f32[16]{0:T(128)S(1)} all-reduce(f32[16]{0:T(128)S(1)} %multiply_reduce_fusion.1), channel_id=1, replica_groups=mesh['ep'=16,'tp'=2] {'tp'}, use_global_device_ids=true, to_apply=%region_9.10 | all-reduce | flops 16 | bytes 128 | tf_op jit(solution)/shard_map/psum | solution.py:133
  46.7 1.5 multiply_reduce_fusion
  48.4 0.8 reshape.154
  49.2 5.6 %all-to-all-start = ((bf16[16,12,512]{2,1,0:T(8,128)(2,1)}), bf16[16,12,512]{2,1,0:T(8,128)(2,1)S(1)}, u32[]{:S(2)}, u32[]{:S(2)}) async-start(bf16[16,12,512]{2,1,0:T(8,128)(2,1)} %reshape.154), calls=%async_computation.1 | async-start | bytes 524288 | tf_op jit(solution)/shard_map/all_to_all | solution.py:152
  54.9 22.6 %all_gather.11 = bf16[256,512]{1,0:T(8,128)(2,1)S(1)} all-gather(bf16[16,512]{1,0:T(8,128)(2,1)S(1)} %get-tuple-element.6), channel_id=1, replica_groups=mesh['ep'=16,'tp'=2] {'ep'}, dimensions={0}, use_global_device_ids=true | all-gather | bytes 278528 | tf_op jit(solution)/shard_map/all_gather | solution.py:186
  77.5 0.9 fusion.12
  78.6 12.0 %all_gather.10 = bf16[16,12,1024]{2,1,0:T(8,128)(2,1)S(1)} all-gather(bf16[16,12,512]{2,1,0:T(8,128)(2,1)S(1)} %all-to-all-done), channel_id=1, replica_groups=mesh['ep'=16,'tp'=2] {'tp'}, dimensions={2}, use_global_device_ids=true | all-gather | bytes 589824 | tf_op jit(solution)/shard_map/all_gather | solution.py:151
  90.7 1.6 convolution_minimum_fusion
  92.3 2.4 %fusion.6 = bf16[192,512]{1,0:T(8,128)(2,1)} fusion(f32[192,512]{1,0:T(8,128)S(1)} %convolution_minimum_fusion, bf16[192,1024]{1,0:T(8,128)(2,1)S(1)} %reshape.155, bf16[1,1024,512]{2,1,0:T(8,128)(2,1)} %param.40), kind=kOutput, calls=%fused_computation.9 | convolution fusion | flops 202211328 | bytes 2031616 | tf_op jit(solution)/shard_map/dot_general | solution.py:166
  94.7 1.0 dot_general.54
  95.8 1.3 fusion.8
  97.7 2.3 %all-reduce.2.cloned.1.call-done = f32[256,256]{1,0:T(8,128)} async-done(((f32[256,256]{1,0:T(8,128)}), f32[256,256]{1,0:T(8,128)}) %all-reduce.2.cloned.1.call-update) | async-done | bytes 262160 | tf_op jit(solution)/shard_map/psum | solution.py:190
  100.0 2.1 %fusion.22 = f32[256,512]{1,0:T(8,128)} fusion(bf16[128,512]{1,0:T(8,128)(2,1)} %param.44, f32[256,256]{1,0:T(8,128)} %all-reduce.2.cloned.1.call-done), kind=kOutput, calls=%fused_computation.32 | convolution fusion | flops 33751040 | bytes 917504 | tf_op jit(solution)/shard_map/dot_general | solution.py:195
  102.7 17.1 %reduce-scatter.6.cloned.1.call-done = f32[16,12,512]{2,0,1:T(8,128)} async-done(((f32[16,12,1024]{2,0,1:T(8,128)}), f32[16,12,512]{2,0,1:T(8,128)}) %reduce-scatter.6.cloned.1.call-update) | async-done | bytes 393232 | tf_op jit(solution)/shard_map/reduce_scatter | solution.py:170
  119.8 1.0 convert_element_type.76
  120.8 0.8 copy.72
  121.6 5.6 %all-to-all-start.1 = ((bf16[16,12,512]{2,1,0:T(8,128)(2,1)}), bf16[16,12,512]{2,1,0:T(8,128)(2,1)S(1)}, u32[]{:S(2)}, u32[]{:S(2)}) async-start(bf16[16,12,512]{2,1,0:T(8,128)(2,1)} %copy.72), calls=%async_computation.3 | async-start | bytes 524288 | tf_op jit(solution)/shard_map/all_to_all | solution.py:173
  127.2 4.9 %psum.22 = f32[16]{0:T(128)S(1)} all-reduce(f32[16]{0:T(128)S(1)} %copy-done.22), channel_id=1, replica_groups=mesh['ep'=16,'tp'=2] {'tp'}, use_global_device_ids=true, to_apply=%region_15.16 | all-reduce | flops 16 | bytes 128 | tf_op jit(solution)/shard_map/psum | solution.py:136
  132.2 5.0 %all-to-all-done.1 = bf16[16,12,512]{2,1,0:T(8,128)(2,1)S(1)} async-done(((bf16[16,12,512]{2,1,0:T(8,128)(2,1)}), bf16[16,12,512]{2,1,0:T(8,128)(2,1)S(1)}, u32[]{:S(2)}, u32[]{:S(2)}) %all-to-all-start.1) | async-done | bytes 196640 | tf_op jit(solution)/shard_map/all_to_all | solution.py:173
  137.5 41.9 %reduce-scatter.8.cloned.1.call-done = f32[16,512]{1,0:T(8,128)} async-done(((f32[256,512]{1,0:T(8,128)}), f32[16,512]{1,0:T(8,128)}) %reduce-scatter.8.cloned.1.call-update) | async-done | bytes 32784 | tf_op jit(solution)/shard_map/reduce_scatter | solution.py:194
  179.4 1.4 add_convert_fusion
  (105 shorter events, 6.2 us)
Async XLA Ops:
  7.2 20.3 %copy-start = (bf16[16,256,256]{2,1,0:T(8,128)(2,1)S(1)}, bf16[16,256,256]{2,1,0:T(8,128)(2,1)}, u32[]{:S(2)}) copy-start(bf16[16,256,256]{2,1,0:T(8,128)(2,1)} %param.34) | copy-start | bytes 6291460
  7.2 33.7 %reduce-scatter.4.cloned.1.call-start = ((), (), s32[]{:S(2)}) async-start(), calls=%async_computation.5 | async-start | bytes 98304 | tf_op jit(solution)/shard_map/reduce_scatter | solution.py:131
  8.1 16.8 %copy-start.13 = (f32[2,64]{1,0:T(2,128)}, f32[2,64]{1,0:T(2,128)S(1)}, u32[]{:S(2)}) copy-start(f32[2,64]{1,0:T(2,128)S(1)} %mul.233) | copy-start | bytes 1540
  16.6 0.6 copy-start.12
  18.5 2.0 %copy-start.7 = (f32[16,256]{1,0:T(8,128)}, f32[16,256]{1,0:T(8,128)S(1)}, u32[]{:S(2)}) copy-start(f32[16,256]{1,0:T(8,128)S(1)} %fusion.51) | copy-start | bytes 49156
  20.6 4.3 %copy-start.5 = (f32[16,2,2]{2,1,0:T(2,128)}, f32[16,2,2]{2,1,0:T(2,128)S(1)}, u32[]{:S(2)}) copy-start(f32[16,2,2]{2,1,0:T(2,128)S(1)} %copy.67) | copy-start | bytes 772
  24.9 2.3 %copy-start.16 = (f32[2]{0:T(128)S(1)}, f32[2]{0:T(128)}, u32[]{:S(2)}) copy-start(f32[2]{0:T(128)} %param.30) | copy-start | bytes 28
  24.9 3.1 %copy-start.21 = (f32[128]{0:T(128)S(1)}, f32[128]{0:T(128)}, u32[]{:S(2)}) copy-start(f32[128]{0:T(128)} %param.31) | copy-start | bytes 1540
  24.9 3.2 %copy-start.2 = (bf16[256,1024]{1,0:T(8,128)(2,1)S(1)}, bf16[256,1024]{1,0:T(8,128)(2,1)}, u32[]{:S(2)}) copy-start(bf16[256,1024]{1,0:T(8,128)(2,1)} %param.32) | copy-start | bytes 1572868
  27.0 2.0 %copy-start.15 = (s32[16,6]{0,1:T(8,128)S(1)}, s32[16,6]{0,1:T(8,128)}, u32[]{:S(2)}) copy-start(s32[16,6]{0,1:T(8,128)} %param.37) | copy-start | bytes 1156
  27.0 13.9 %copy-start.4 = (bf16[16,512]{1,0:T(8,128)(2,1)S(1)}, bf16[16,512]{1,0:T(8,128)(2,1)}, u32[]{:S(2)}) copy-start(bf16[16,512]{1,0:T(8,128)(2,1)} %param.23) | copy-start | bytes 49156
  27.0 19.7 %copy-start.19 = (f32[512]{0:T(512)S(1)}, f32[512]{0:T(512)}, u32[]{:S(2)}) copy-start(f32[512]{0:T(512)} %param.45) | copy-start | bytes 6148
  27.0 19.7 %copy-start.20 = (f32[512]{0:T(512)S(1)}, f32[512]{0:T(512)}, u32[]{:S(2)}) copy-start(f32[512]{0:T(512)} %param.36) | copy-start | bytes 6148
  27.5 50.1 %copy-start.9 = (bf16[512,128]{1,0:T(8,128)(2,1)S(1)}, bf16[512,128]{1,0:T(8,128)(2,1)}, u32[]{:S(2)}) copy-start(bf16[512,128]{1,0:T(8,128)(2,1)} %param.43) | copy-start | bytes 393220
  27.5 50.1 %copy-start.10 = (bf16[512,128]{1,0:T(8,128)(2,1)S(1)}, bf16[512,128]{1,0:T(8,128)(2,1)}, u32[]{:S(2)}) copy-start(bf16[512,128]{1,0:T(8,128)(2,1)} %param.42) | copy-start | bytes 393220
  29.6 49.0 %copy-start.17 = (s32[96]{0:T(128)}, s32[96]{0:T(128)S(1)}, u32[]{:S(2)}) copy-start(s32[96]{0:T(128)S(1)} %multiply_add_fusion.1) | copy-start | bytes 1156
  49.2 29.4 %all-to-all-start = ((bf16[16,12,512]{2,1,0:T(8,128)(2,1)}), bf16[16,12,512]{2,1,0:T(8,128)(2,1)S(1)}, u32[]{:S(2)}, u32[]{:S(2)}) async-start(bf16[16,12,512]{2,1,0:T(8,128)(2,1)} %reshape.154), calls=%async_computation.1 | async-start | bytes 524288 | tf_op jit(solution)/shard_map/all_to_all | solution.py:152
  54.8 45.1 %all-reduce.2.cloned.1.call-start = ((), (), s32[]{:S(2)}) async-start(), calls=%async_computation.7 | async-start | bytes 524288 | tf_op jit(solution)/shard_map/psum | solution.py:190
  78.5 41.3 %reduce-scatter.6.cloned.1.call-start = ((), (), s32[]{:S(2)}) async-start(), calls=%async_computation.6 | async-start | bytes 1179648 | tf_op jit(solution)/shard_map/reduce_scatter | solution.py:170
  92.3 3.5 %copy-start.1 = (bf16[1,512,1024]{2,1,0:T(8,128)(2,1)S(1)}, bf16[1,512,1024]{2,1,0:T(8,128)(2,1)}, u32[]{:S(2)}) copy-start(bf16[1,512,1024]{2,1,0:T(8,128)(2,1)} %param.41) | copy-start | bytes 3145732
  94.7 2.5 %copy-start.14 = (f32[2,64]{1,0:T(2,128)S(1)}, f32[2,64]{1,0:T(2,128)}, u32[]{:S(2)}) copy-start(f32[2,64]{1,0:T(2,128)} %copy-done.13) | copy-start | bytes 1540
  94.7 2.6 %copy-start.6 = (f32[16,2,2]{2,1,0:T(2,128)S(1)}, f32[16,2,2]{2,1,0:T(2,128)}, u32[]{:S(2)}) copy-start(f32[16,2,2]{2,1,0:T(2,128)} %copy-done.5) | copy-start | bytes 772
  94.7 2.8 %copy-start.18 = (s32[96]{0:T(128)S(1)}, s32[96]{0:T(128)}, u32[]{:S(2)}) copy-start(s32[96]{0:T(128)} %copy-done.17) | copy-start | bytes 1156
  94.7 2.9 %copy-start.11 = (f32[16,6]{0,1:T(8,128)S(1)}, f32[16,6]{0,1:T(8,128)}, u32[]{:S(2)}) copy-start(f32[16,6]{0,1:T(8,128)} %param.38) | copy-start | bytes 1156
  95.8 6.3 %copy-start.8 = (f32[16,256]{1,0:T(8,128)S(1)}, f32[16,256]{1,0:T(8,128)}, u32[]{:S(2)}) copy-start(f32[16,256]{1,0:T(8,128)} %copy-done.7) | copy-start | bytes 49156
  97.1 30.1 %copy-start.22 = (f32[16]{0:T(128)S(1)}, f32[16]{0:T(128)}, u32[]{:S(2)}) copy-start(f32[16]{0:T(128)} %get-tuple-element.5) | copy-start | bytes 196
  97.1 82.3 %copy-start.3 = (f32[16,512]{1,0:T(8,128)S(1)}, f32[16,512]{1,0:T(8,128)}, u32[]{:S(2)}) copy-start(f32[16,512]{1,0:T(8,128)} %reduce-scatter.4.cloned.1.call-done) | copy-start | bytes 98308
  97.1 82.2 %reduce-scatter.8.cloned.1.call-start = ((), (), s32[]{:S(2)}) async-start(), calls=%async_computation.8 | async-start | bytes 557056 | tf_op jit(solution)/shard_map/reduce_scatter | solution.py:194
  121.6 15.6 %all-to-all-start.1 = ((bf16[16,12,512]{2,1,0:T(8,128)(2,1)}), bf16[16,12,512]{2,1,0:T(8,128)(2,1)S(1)}, u32[]{:S(2)}, u32[]{:S(2)}) async-start(bf16[16,12,512]{2,1,0:T(8,128)(2,1)} %copy.72), calls=%async_computation.3 | async-start | bytes 524288 | tf_op jit(solution)/shard_map/all_to_all | solution.py:173
Sparse Core Ops, SparseCore 0:
  29.1 11.6 reduce-scatter.3
  78.6 21.3 all-reduce.1
  102.2 17.4 reduce-scatter.5
  123.2 56.1 reduce-scatter.7
where the time goes:
time: 188 us; the launch traced here: 187 us
  waiting for transfers between devices  77.7 us (41%)
  blocking collectives  50.2 us (27%)
  matrix products  15.7 us (8%)
  between operations  14.2 us (8%)
  starting transfers between devices  11.4 us (6%)
  local copies, waits for them, and re-layouts  10.2 us (5%)
  other arithmetic  7.98 us (4%)
    reduce_scatter x1, waiting for transfers between devices, body(): lax.psum_scatter(jnp.dot(all_act, dense_down, preferred_element_type=jnp....  41.9 us
    all_gather x1, blocking collectives, body(): lax.all_gather(mix_rows, 'ep', axis=0, tiled=True)  22.6 us
    reduce_scatter x1, waiting for transfers between devices, body(): lax.psum_scatter(partial_out, 'tp', scatter_dimension=2, tiled=True)  17.1 us
    all_gather x1, blocking collectives, body(): lax.all_gather(lax.all_to_all(placed.astype(jnp.bfloat16).reshape(experts...  12 us
    reduce_scatter x1, waiting for transfers between devices, body(): lax.psum_scatter(head_terms, 'tp', scatter_dimension=1, tiled=True)  11.3 us
    all_to_all x1, starting transfers between devices, body(): lax.all_to_all(placed.astype(jnp.bfloat16).reshape(experts, capacity, mix...  5.63 us
    all_gather x1, blocking collectives, body(): full_rows = lax.all_gather(hidden_in, 'tp', axis=1, tiled=True)  5.63 us
    all_to_all x1, starting transfers between devices, body(): lax.all_to_all(summed, 'ep', split_axis=0, concat_axis=0, tiled=True)  5.62 us
  transfers between devices with their start and end apart: 6, of which 5 were waited for; matrix products, arithmetic and copies ran while one was open for 7% of the time, Pallas kernels for 0%

commit v1 on v0

v1 whole, which is shorter than its diff:
```python
import functools
import math

import jax
import jax.numpy as jnp
from jax import lax
from jax.experimental import pallas as pl
from jax.experimental.pallas import tpu as pltpu
from jax.sharding import PartitionSpec as P

EPSILON = 1e-06
CLAMP_LIMIT = 7.0
SWISH_ALPHA = 1.702
OUT_SCALE = 0.2 + 0.6 * math.exp(-0.6)
F32 = jnp.float32
BF16 = jnp.bfloat16
MESH = pl.DeviceIdType.MESH


def dot(a, b):
    return jnp.dot(a, b, preferred_element_type=F32)


def group_rms(values, gain, group):
    lane = lax.broadcasted_iota(jnp.int32, values.shape, 1)
    squares = values * values
    scale = jnp.zeros_like(values)
    for g in range(values.shape[1] // group):
        inside = (lane >= g * group) & (lane < (g + 1) * group)
        total = jnp.sum(jnp.where(inside, squares, 0.0), axis=1, keepdims=True)
        scale = jnp.where(inside, lax.rsqrt(total / group + EPSILON), scale)
    return values * scale * gain


def layer_kernel(
    n_ep,
    n_tp,
    lam_ref,
    len_ref,
    hid_ref,
    gain_attn_ref,
    qg_ref,
    kg_ref,
    sub_ref,
    gain_mix_ref,
    branch_ref,
    ids_ref,
    logits_ref,
    wq_hbm,
    wk_hbm,
    wv_hbm,
    wo_hbm,
    ck_hbm,
    cv_hbm,
    eg_hbm,
    eu_hbm,
    ed_hbm,
    dg_hbm,
    du_hbm,
    dd_hbm,
    out_ref,
    key_ref,
    val_ref,
    wq,
    wk,
    wv,
    wo,
    ck,
    cv,
    eg,
    eu,
    ed,
    dgbuf,
    dubuf,
    dd,
    hbuf,
    gbuf,
    bbuf,
    vrow,
    hout,
    res,
    abuf,
    gath,
    ybuf,
    ysend,
    pbuf,
    sbuf,
    rbuf,
    lsem,
    tp_send,
    tp_recv,
    g_send,
    f_send,
    g_recv,
    p_sem,
    r_send,
    r_recv,
):
    e = lax.axis_index("ep")
    t = lax.axis_index("tp")
    chips = n_ep // 2
    chip = lax.div(e, 2)
    core = lax.rem(e, 2)
    sib = chip * 2 + (1 - core)
    n_all = chips * n_tp
    rows, half = hid_ref.shape
    width = half * n_tp

    loads = []
    for i, (src, dst) in enumerate(
        [
            (wq_hbm, wq),
            (wk_hbm, wk),
            (wv_hbm, wv),
            (ck_hbm, ck),
            (cv_hbm, cv),
            (wo_hbm, wo),
            (dg_hbm, dgbuf.at[t]),
            (du_hbm, dubuf.at[t]),
            (eg_hbm.at[0], eg),
            (eu_hbm.at[0], eu),
            (ed_hbm.at[0], ed),
            (dd_hbm, dd),
        ]
    ):
        copy = pltpu.make_async_copy(src, dst, lsem.at[i])
        copy.start()
        loads.append(copy)

    barrier = pltpu.get_barrier_semaphore()
    me = t * chips + chip

    def greet(i, carry):
        other = lax.rem(me + i, n_all)
        pl.semaphore_signal(
            barrier,
            inc=1,
            device_id={"ep": lax.rem(other, chips) * 2 + core, "tp": lax.div(other, chips)},
            device_id_type=MESH,
        )
        return carry

    lax.fori_loop(1, n_all, greet, 0)
    pl.semaphore_signal(barrier, inc=1, device_id={"ep": sib, "tp": t}, device_id_type=MESH)

    hbuf[t] = hid_ref[...]
    gbuf[t] = gain_mix_ref[...]
    bbuf[t] = branch_ref[...]

    ext = gath.shape[2] - width
    logits = logits_ref[...]
    top = logits - jnp.max(logits, axis=1, keepdims=True)
    expo = jnp.exp(top)
    route = expo / jnp.sum(expo, axis=1, keepdims=True)
    ids = ids_ref[...]
    lane = lax.broadcasted_iota(jnp.int32, (rows, ext), 1)
    first = lane <= n_ep
    lane_id = jnp.where(first, lane, lane - (n_ep + 1))
    table = jnp.zeros((rows, ext), F32)
    for k in range(ids.shape[1]):
        table = table + jnp.where(lane_id == ids[:, k : k + 1], route[:, k : k + 1], 0.0)

    pl.semaphore_wait(barrier, n_all)

    def tp_copies(kind, src, dst_ref):
        sends = []
        for d in range(1, n_tp):
            peer = lax.rem(t + d, n_tp)
            copy = pltpu.make_async_remote_copy(
                src_ref=src,
                dst_ref=dst_ref.at[t],
                send_sem=tp_send.at[kind, d - 1],
                recv_sem=tp_recv.at[kind, t],
                device_id={"ep": e, "tp": peer},
                device_id_type=MESH,
            )
            copy.start()
            sends.append(copy)
        return sends

    def tp_arrive(kind, src, dst_ref):
        for d in range(1, n_tp):
            peer = lax.rem(t + d, n_tp)
            pltpu.make_async_remote_copy(
                src_ref=src,
                dst_ref=dst_ref.at[peer],
                send_sem=tp_send.at[kind, d - 1],
                recv_sem=tp_recv.at[kind, peer],
                device_id={"ep": e, "tp": peer},
                device_id_type=MESH,
            ).wait_recv()

    pending = []
    pending += tp_copies(0, hid_ref, hbuf)
    pending += tp_copies(1, gain_mix_ref, gbuf)
    pending += tp_copies(2, branch_ref, bbuf)

    tp_arrive(0, hid_ref, hbuf)
    hidden = [hbuf[j].astype(F32) for j in range(n_tp)]
    square = sum(jnp.sum(h * h, axis=1, keepdims=True) for h in hidden)
    inverse = lax.rsqrt(square / width + EPSILON)
    normed = [
        (hidden[j] * inverse * gain_attn_ref[:, j * half : (j + 1) * half]).astype(BF16)
        for j in range(n_tp)
    ]

    def project(w):
        return sum(dot(normed[j], w[j * half : (j + 1) * half, :]) for j in range(n_tp))

    qk2 = qg_ref.shape[1]
    qk = qk2 // 2
    cols = wq.shape[1]
    heads = cols // qk2
    val = sub_ref.shape[1]
    q_gain = jnp.concatenate([qg_ref[...]] * heads, axis=1)
    k_gain = jnp.concatenate([kg_ref[...]] * heads, axis=1)
    sub_gain = jnp.concatenate([sub_ref[...]] * heads, axis=1)
    loads[0].wait()
    q_rows = group_rms(project(wq), q_gain, qk).astype(BF16).astype(F32)
    loads[1].wait()
    k_bf = group_rms(project(wk), k_gain, qk).astype(BF16)
    k_rows = k_bf.astype(F32)
    loads[2].wait()
    v_bf = project(wv).astype(BF16)
    key_ref[...] = k_bf
    val_ref[...] = v_bf
    vrow[...] = v_bf.astype(F32)

    qcol = lax.broadcasted_iota(jnp.int32, (16, cols), 1)
    qrow = lax.broadcasted_iota(jnp.int32, (16, cols), 0)
    inside = (qcol // qk) == (2 * (qrow % 8) + qrow // 8)
    vcol = lax.broadcasted_iota(jnp.int32, (8, heads * val), 1)
    vhead = lax.broadcasted_iota(jnp.int32, (8, heads * val), 0)
    own_head = (vcol // val) == vhead
    lrow = lax.broadcasted_iota(jnp.int32, (8, 1), 0)
    lam = jnp.zeros((8, 1), F32)
    for h in range(heads):
        lam = jnp.where(lrow == h, lam_ref[h], lam)
    factor = qk ** (-0.5)
    cache_len = ck.shape[1]
    pos = lax.broadcasted_iota(jnp.int32, (16, cache_len), 1)
    loads[3].wait()
    loads[4].wait()
    for s in range(rows):
        q_s = jnp.where(inside, q_rows[s : s + 1, :], 0.0)
        own = jnp.exp(jnp.sum(q_s * k_rows[s : s + 1, :], axis=1, keepdims=True) * factor)
        score = lax.dot_general(
            q_s.astype(BF16), ck[s], (((1,), (1,)), ((), ())), preferred_element_type=F32
        )
        past = jnp.where(pos < len_ref[s], jnp.exp(score * factor), 0.0)
        inv_den = 1.0 / (jnp.sum(past, axis=1, keepdims=True) + own)
        prob = past * inv_den
        own = own * inv_den
        weight = (prob[:8] - lam * prob[8:]).astype(BF16)
        weight_own = (own[:8] - lam * own[8:]).astype(BF16).astype(F32)
        mix = dot(weight, cv[s]) + weight_own * vrow[s : s + 1, :]
        mix = jnp.where(own_head, mix, 0.0)
        square = jnp.sum(mix * mix, axis=1, keepdims=True)
        mix = mix * lax.rsqrt(square / val + EPSILON) * sub_gain * OUT_SCALE
        hout[s : s + 1, :] = jnp.sum(mix, axis=0, keepdims=True)
    loads[5].wait()
    attn = dot(hout[...].astype(BF16), wo[...])
    abuf[t] = attn.astype(BF16)
    pending += tp_copies(3, abuf.at[t], abuf)
    loads[6].wait()
    loads[7].wait()
    pending += tp_copies(4, dgbuf.at[t], dgbuf)
    pending += tp_copies(5, dubuf.at[t], dubuf)
    tp_arrive(1, gain_mix_ref, gbuf)
    tp_arrive(2, branch_ref, bbuf)
    tp_arrive(3, abuf.at[t], abuf)

    for d in range(1, n_tp):
        attn = attn + abuf[lax.rem(t + d, n_tp)].astype(F32)
    slot = core * chips + chip
    square = jnp.zeros((rows, 1), F32)
    total = []
    for j in range(n_tp):
        r = hbuf[j].astype(F32) + attn[:, j * half : (j + 1) * half]
        res[j] = r
        total.append(r)
        square = square + jnp.sum(r * r, axis=1, keepdims=True)
    inverse = lax.rsqrt(square / width + EPSILON)
    logit = jnp.zeros((rows, 1), F32)
    for j in range(n_tp):
        m = total[j] * inverse * gbuf[j]
        logit = logit + jnp.sum(m * bbuf[j], axis=1, keepdims=True)
        gath[slot, :, j * half : (j + 1) * half] = m.astype(BF16)
    branch = 1.0 / (1.0 + jnp.exp(-logit))
    table = jnp.where(lane_id == n_ep, branch, table)
    high = table.astype(BF16).astype(F32)
    gath[slot, :, width:] = jnp.where(first, high, table - high).astype(BF16)

    def gather_copy(at, send, ep_to):
        return pltpu.make_async_remote_copy(
            src_ref=gath.at[at],
            dst_ref=gath.at[at],
            send_sem=send,
            recv_sem=g_recv.at[at],
            device_id={"ep": ep_to, "tp": t},
            device_id_type=MESH,
        )

    def scatter(i, carry):
        to = lax.rem(chip + i, chips)
        gather_copy(slot, g_send.at[i], to * 2 + core).start()
        return carry

    lax.fori_loop(1, chips, scatter, 0)
    gather_copy(slot, g_send.at[0], sib).start()

    def forward(i, carry):
        at = core * chips + lax.rem(chip + chips - i, chips)
        gather_copy(at, f_send.at[i], sib).wait_recv()
        gather_copy(at, f_send.at[i], sib).start()
        return carry

    lax.fori_loop(1, chips, forward, 0)

    for i in range(8, 12):
        loads[i].wait()
    tp_arrive(4, dgbuf.at[t], dgbuf)
    tp_arrive(5, dubuf.at[t], dubuf)

    def expert(par):
        x = gath[pl.ds(par * chips, chips), :, :].reshape(chips * rows, width + ext)
        tokens = x[:, :width]
        extra = x[:, width:].astype(F32)
        place = lax.broadcasted_iota(jnp.int32, extra.shape, 1)
        mine = (place == e) | (place == e + n_ep + 1)
        w_route = jnp.sum(jnp.where(mine, extra, 0.0), axis=1, keepdims=True)
        dense_at = (place == n_ep) | (place == 2 * n_ep + 1)
        w_dense = jnp.sum(jnp.where(dense_at, extra, 0.0), axis=1, keepdims=True)
        gate = jnp.minimum(dot(tokens, eg[...]), CLAMP_LIMIT)
        up = jnp.clip(dot(tokens, eu[...]), -CLAMP_LIMIT, CLAMP_LIMIT)
        act = ((up + 1.0) * gate / (1.0 + jnp.exp(-SWISH_ALPHA * gate))).astype(BF16)
        dg = sum(dot(tokens[:, j * half : (j + 1) * half], dgbuf[j]) for j in range(n_tp))
        du = sum(dot(tokens[:, j * half : (j + 1) * half], dubuf[j]) for j in range(n_tp))
        dact = (dg / (1.0 + jnp.exp(-dg)) * du).astype(BF16)
        dense = dot(dact, dd[...]) * w_dense
        parts = []
        for j in range(n_tp):
            y = dot(act, ed[:, j * half : (j + 1) * half]) * w_route
            parts.append((y + jnp.where(t == j, dense, 0.0)).reshape(chips, rows, half))
        return parts

    own_parts = expert(core)
    for j in range(n_tp):
        ybuf[j] = own_parts[j]

    def arrived(i, carry):
        at = (1 - core) * chips + i
        gather_copy(at, g_send.at[0], sib).wait_recv()
        return carry

    lax.fori_loop(0, chips, arrived, 0)
    sib_parts = expert(1 - core)
    for j in range(n_tp):
        ysend[j] = sib_parts[j].astype(BF16)
    pair = pltpu.make_async_remote_copy(
        src_ref=ysend,
        dst_ref=pbuf,
        send_sem=p_sem.at[0],
        recv_sem=p_sem.at[1],
        device_id={"ep": sib, "tp": t},
        device_id_type=MESH,
    )
    pair.start()
    pair.wait_recv()
    for j in range(n_tp):
        both = ybuf[j] + pbuf[j].astype(F32)
        sbuf[j] = both.astype(BF16)

    def result_copy(i, to_t, to_chip, from_t, from_chip):
        return pltpu.make_async_remote_copy(
            src_ref=sbuf.at[to_t, to_chip],
            dst_ref=rbuf.at[from_t, from_chip],
            send_sem=r_send.at[i],
            recv_sem=r_recv.at[from_t * chips + from_chip],
            device_id={"ep": to_chip * 2 + core, "tp": to_t},
            device_id_type=MESH,
        )

    def give(i, carry):
        to = lax.rem(me + i, n_all)
        result_copy(i, lax.div(to, chips), lax.rem(to, chips), t, chip).start()
        return carry

    lax.fori_loop(1, n_all, give, 0)
    final = res[t] + ybuf[t, chip] + pbuf[t, chip].astype(F32)

    def take(i, total):
        src = lax.rem(me + n_all - i, n_all)
        src_t, src_chip = lax.div(src, chips), lax.rem(src, chips)
        result_copy(i, t, chip, src_t, src_chip).wait_recv()
        return total + rbuf[src_t, src_chip].astype(F32)

    final = lax.fori_loop(1, n_all, take, final)
    out_ref[...] = final.astype(BF16)

    for copy in pending:
        copy.wait_send()
    pair.wait_send()

    def drain_gather(i, carry):
        gather_copy(slot, g_send.at[i], sib).wait_send()
        return carry

    lax.fori_loop(0, chips, drain_gather, 0)

    def drain_forward(i, carry):
        gather_copy(slot, f_send.at[i], sib).wait_send()
        return carry

    lax.fori_loop(1, chips, drain_forward, 0)

    def drain_result(i, carry):
        to = lax.rem(me + i, n_all)
        result_copy(i, lax.div(to, chips), lax.rem(to, chips), t, chip).wait_send()
        return carry

    lax.fori_loop(1, n_all, drain_result, 0)


def body(
    n_ep,
    n_tp,
    hidden_in,
    norm_gain_attn,
    query_weight,
    key_weight,
    value_weight,
    query_gain,
    key_gain,
    lambda_head,
    sub_gain,
    out_weight,
    cache_key,
    cache_value,
    lengths,
    norm_gain_mix,
    route_ids,
    route_logits,
    expert_gate,
    expert_up,
    expert_down,
    dense_gate,
    dense_up,
    dense_down,
    branch_gate,
):
    rows, half = hidden_in.shape
    width = half * n_tp
    chips = n_ep // 2
    n_all = chips * n_tp
    ext = -(-2 * (n_ep + 1) // 128) * 128
    smem = pl.BlockSpec(memory_space=pltpu.SMEM)
    vmem = pl.BlockSpec(memory_space=pltpu.VMEM)
    hbm = pl.BlockSpec(memory_space=pl.ANY)
    dma = pltpu.SemaphoreType.DMA
    cols = query_weight.shape[1]
    vcols = value_weight.shape[1]
    block = (n_tp, chips, rows, half)
    scratch = [
        pltpu.VMEM(query_weight.shape, BF16),
        pltpu.VMEM(key_weight.shape, BF16),
        pltpu.VMEM(value_weight.shape, BF16),
        pltpu.VMEM(out_weight.shape, BF16),
        pltpu.VMEM(cache_key.shape, BF16),
        pltpu.VMEM(cache_value.shape, BF16),
        pltpu.VMEM(expert_gate.shape[1:], BF16),
        pltpu.VMEM(expert_up.shape[1:], BF16),
        pltpu.VMEM(expert_down.shape[1:], BF16),
        pltpu.VMEM((n_tp,) + dense_gate.shape, BF16),
        pltpu.VMEM((n_tp,) + dense_up.shape, BF16),
        pltpu.VMEM(dense_down.shape, BF16),
        pltpu.VMEM((n_tp, rows, half), BF16),
        pltpu.VMEM((n_tp, 1, half), F32),
        pltpu.VMEM((n_tp, 1, half), F32),
        pltpu.VMEM((rows, vcols), F32),
        pltpu.VMEM((rows, vcols), F32),
        pltpu.VMEM((n_tp, rows, half), F32),
        pltpu.VMEM((n_tp, rows, width), BF16),
        pltpu.VMEM((n_ep, rows, width + ext), BF16),
        pltpu.VMEM(block, F32),
        pltpu.VMEM(block, BF16),
        pltpu.VMEM(block, BF16),
        pltpu.VMEM(block, BF16),
        pltpu.VMEM(block, BF16),
        dma((12,)),
        dma((6, n_tp)),
        dma((6, n_tp)),
        dma((chips,)),
        dma((chips,)),
        dma((n_ep,)),
        dma((2,)),
        dma((n_all,)),
        dma((n_all,)),
    ]
    return pl.pallas_call(
        functools.partial(layer_kernel, n_ep, n_tp),
        out_shape=(
            jax.ShapeDtypeStruct((rows, half), BF16),
            jax.ShapeDtypeStruct((rows, cols), BF16),
            jax.ShapeDtypeStruct((rows, vcols), BF16),
        ),
        in_specs=[smem] * 2 + [vmem] * 9 + [hbm] * 12,
        out_specs=(vmem, vmem, vmem),
        scratch_shapes=scratch,
        compiler_params=pltpu.CompilerParams(
            collective_id=0, has_side_effects=True, vmem_limit_bytes=56 * 1024 * 1024
        ),
    )(
        lambda_head,
        lengths,
        hidden_in,
        norm_gain_attn.reshape(1, -1),
        query_gain.reshape(1, -1),
        key_gain.reshape(1, -1),
        sub_gain.reshape(1, -1),
        norm_gain_mix.reshape(1, -1),
        branch_gate.reshape(1, -1),
        route_ids,
        route_logits,
        query_weight,
        key_weight,
        value_weight,
        out_weight,
        cache_key,
        cache_value,
        expert_gate,
        expert_up,
        expert_down,
        dense_gate,
        dense_up,
        dense_down,
    )


def solution(mesh):
    in_specs = (
        P("ep", "tp"),
        P(),
        P(None, "tp"),
        P(None, "tp"),
        P(None, "tp"),
        P(),
        P(),
        P("tp"),
        P(),
        P("tp", None),
        P("ep", None, "tp"),
        P("ep", None, "tp"),
        P("ep"),
        P("tp"),
        P("ep", None),
        P("ep", None),
        P("ep", None, "tp"),
        P("ep", None, "tp"),
        P("ep", "tp", None),
        P("tp", "ep"),
        P("tp", "ep"),
        P("ep", "tp"),
        P("tp"),
    )
    out_specs = (P("ep", "tp"), P("ep", "tp"), P("ep", "tp"))
    step = functools.partial(body, mesh.shape["ep"], mesh.shape["tp"])
    return jax.shard_map(step, mesh=mesh, in_specs=in_specs, out_specs=out_specs, check_vma=False)
```

time: 188 us -> 45.4 us (0.24)
  waiting for transfers between devices: 77.7 us -> 0 us
  blocking collectives: 50.2 us -> 0 us
  Pallas kernels: 0 us -> 37.6 us
  matrix products: 15.7 us -> 0 us
  between operations: 14.2 us -> 0.64 us
  starting transfers between devices: 11.4 us -> 0 us
  other arithmetic: 7.98 us -> 0 us
  local copies, waits for them, and re-layouts: 10.2 us -> 6.64 us
    reduce_scatter x3 -> x0, waiting for transfers between devices: 70.3 us -> none  [the longest x1 41.9 us: body(): lax.psum_scatter(jnp.dot(all_act, dense_down, preferred_element_type=jnp....]
    all_gather x3 -> x0, blocking collectives: 40.3 us -> none  [the longest x1 22.6 us: body(): lax.all_gather(mix_rows, 'ep', axis=0, tiled=True)]
    pallas_call x0 -> x1, Pallas kernels: none -> 37.6 us  [body(): pl.pallas_call(functools.partial(layer_kernel, n_ep, n_tp), out_shape=(ja...]
    dot_general x13 -> x0, matrix products: 15.7 us -> none  [the longest x1 2.41 us: body(): jnp.dot(flat_rows, expert_up[0], preferred_element_type=jnp.float32)]
    all_to_all x2 -> x0, starting transfers between devices: 11.3 us -> none  [the longest x1 5.63 us: body(): lax.all_to_all(placed.astype(jnp.bfloat16).reshape(experts, capacity, mix...]
    psum x2 -> x0, blocking collectives: 9.86 us -> none  [the longest x1 4.93 us: body(): lax.psum(jnp.sum(mix_float * branch_gate[None, :], axis=1), 'tp')]
    all_to_all x2 -> x0, waiting for transfers between devices: 5.05 us -> none  [the longest x1 5.04 us: body(): lax.all_to_all(summed, 'ep', split_axis=0, concat_axis=0, tiled=True)]
    convert_element_type x6 -> x0, other arithmetic: 3.33 us -> none  [the longest x1 1.44 us: body(): (residual + routed + branch_weight * dense_result).astype(jnp.bfloat16)]
  transfers between devices with their start and end apart: 6 -> 0, of which waited for: 5 -> 0; matrix products, arithmetic and copies ran while one was open for 7% -> 0% of each run, Pallas kernels for 0% -> 0%
where the time goes in v1:
time: 45.4 us; the launch traced here: 44.9 us
  Pallas kernels  37.6 us (83%)
  local copies, waits for them, and re-layouts  6.64 us (15%)
  between operations  0.64 us (1%)
    pallas_call x1, Pallas kernels, body(): pl.pallas_call(functools.partial(layer_kernel, n_ep, n_tp), out_shape=(ja...  37.6 us
    unnamed x5, local copies, waits for them, and re-layouts  6.64 us

profile of v1, /device:TPU:0, one launch (start us, length us, event | category | flops | bytes accessed | tf_op | source)
XLA Modules:
  0.0 44.9 jit_solution(18310944943600554289)
XLA Ops:
  0.6 1.4 %copy.26.ids_ref = s32[16,6]{1,0:T(8,128)} copy(s32[16,6]{0,1:T(8,128)} %param.37) | data formatting | bytes 768 | tf_op args[14]
  2.0 1.4 %copy.27.logits_ref = f32[16,6]{1,0:T(8,128)} copy(f32[16,6]{0,1:T(8,128)} %param.38) | data formatting | bytes 768 | tf_op args[15]
  3.4 37.6 %shard_map.238 = (bf16[16,512]{1,0:T(8,128)(2,1)}, bf16[16,256]{1,0:T(8,128)(2,1)}, bf16[16,256]{1,0:T(8,128)(2,1)}) custom-call(f32[2]{0:T(128)} %lam_ref.1, s32[16]{0:T(128)} %len_ref.1, bf16[16,512]{1,0:T(8,128)(2,1)} %hid_ref.1, f32[1,1024]{1,0:T(1,128)} %bitcast.6, f32[1,128]{1,0:T(1,128)} %bitcast.9, f32[1,128]{1,0:T(1,128)} %bitcast.10, ...), custom_call_target="tpu_custom_call" | custom-call | tf_op jit(solution)/shard_map/pallas_call | solution.py:500
  41.0 1.3 %copy.31 = bf16[16,512]{1,0:T(8,128)(2,1)} copy(bf16[16,512]{1,0:T(8,128)(2,1)} %get-tuple-element.6) | data formatting | bytes 32768
  42.3 1.3 %copy.32 = bf16[16,256]{1,0:T(8,128)(2,1)} copy(bf16[16,256]{1,0:T(8,128)(2,1)} %get-tuple-element.7) | data formatting | bytes 16384
  43.6 1.3 %copy.33 = bf16[16,256]{1,0:T(8,128)(2,1)} copy(bf16[16,256]{1,0:T(8,128)(2,1)} %get-tuple-element.8) | data formatting | bytes 16384

commit v2 on v1

--- a/solution.py
+++ b/solution.py
@@ -30,6 +30,12 @@
         total = jnp.sum(jnp.where(inside, squares, 0.0), axis=1, keepdims=True)
         scale = jnp.where(inside, lax.rsqrt(total / group + EPSILON), scale)
     return values * scale * gain
+
+
+def hand_on(a_ref, b_ref, c_ref, a_out, b_out, c_out):
+    a_out[...] = a_ref[...]
+    b_out[...] = b_ref[...]
+    c_out[...] = c_ref[...]
 
 
 def layer_kernel(
@@ -148,17 +154,27 @@
     bbuf[t] = branch_ref[...]
 
     ext = gath.shape[2] - width
+    def split(table, first):
+        high = table.astype(BF16).astype(F32)
+        return jnp.where(first, high, table - high)
+
     logits = logits_ref[...]
-    top = logits - jnp.max(logits, axis=1, keepdims=True)
+    top = logits - jnp.max(logits, axis=0, keepdims=True)
     expo = jnp.exp(top)
-    route = expo / jnp.sum(expo, axis=1, keepdims=True)
+    route = expo / jnp.sum(expo, axis=0, keepdims=True)
     ids = ids_ref[...]
-    lane = lax.broadcasted_iota(jnp.int32, (rows, ext), 1)
-    first = lane <= n_ep
-    lane_id = jnp.where(first, lane, lane - (n_ep + 1))
-    table = jnp.zeros((rows, ext), F32)
-    for k in range(ids.shape[1]):
-        table = table + jnp.where(lane_id == ids[:, k : k + 1], route[:, k : k + 1], 0.0)
+    place = lax.broadcasted_iota(jnp.int32, (ext, rows), 0)
+    place_id = jnp.where(place <= n_ep, place, place - (n_ep + 1))
+    table = jnp.zeros((ext, rows), F32)
+    for k in range(ids.shape[0]):
+        table = table + jnp.where(place_id == ids[k : k + 1, :], route[k : k + 1, :], 0.0)
+    table = split(table, place <= n_ep).astype(BF16)
+    unit = lax.broadcasted_iota(jnp.int32, (rows, rows), 0) == lax.broadcasted_iota(
+        jnp.int32, (rows, rows), 1
+    )
+    table = lax.dot_general(
+        unit.astype(F32).astype(BF16), table, (((1,), (1,)), ((), ())), preferred_element_type=F32
+    )
 
     pl.semaphore_wait(barrier, n_all)
 
@@ -287,9 +303,10 @@
         logit = logit + jnp.sum(m * bbuf[j], axis=1, keepdims=True)
         gath[slot, :, j * half : (j + 1) * half] = m.astype(BF16)
     branch = 1.0 / (1.0 + jnp.exp(-logit))
-    table = jnp.where(lane_id == n_ep, branch, table)
-    high = table.astype(BF16).astype(F32)
-    gath[slot, :, width:] = jnp.where(first, high, table - high).astype(BF16)
+    lane = lax.broadcasted_iota(jnp.int32, (rows, ext), 1)
+    at_branch = (lane == n_ep) | (lane == 2 * n_ep + 1)
+    table = jnp.where(at_branch, split(branch, lane <= n_ep), table)
+    gath[slot, :, width:] = table.astype(BF16)
 
     def gather_copy(at, send, ep_to):
         return pltpu.make_async_remote_copy(
@@ -301,21 +318,39 @@
             device_id_type=MESH,
         )
 
+    columns = chips // 2
+    column = lax.div(chip, 2)
+    side = lax.rem(chip, 2)
+    beside = (column * 2 + (1 - side)) * 2 + core
+
     def scatter(i, carry):
-        to = lax.rem(chip + i, chips)
+        to = lax.rem(column + i, columns) * 2 + side
         gather_copy(slot, g_send.at[i], to * 2 + core).start()
         return carry
 
-    lax.fori_loop(1, chips, scatter, 0)
-    gather_copy(slot, g_send.at[0], sib).start()
+    lax.fori_loop(1, columns, scatter, 0)
+    gather_copy(slot, f_send.at[0], beside).start()
+    gather_copy(slot, f_send.at[columns], sib).start()
+
+    def source(i, of_side):
+        return core * chips + lax.rem(column + columns - i, columns) * 2 + of_side
 
     def forward(i, carry):
-        at = core * chips + lax.rem(chip + chips - i, chips)
-        gather_copy(at, f_send.at[i], sib).wait_recv()
-        gather_copy(at, f_send.at[i], sib).start()
-        return carry
-
-    lax.fori_loop(1, chips, forward, 0)
+        at = source(i, side)
+        gather_copy(at, f_send.at[i], beside).wait_recv()
+        gather_copy(at, f_send.at[i], beside).start()
+        gather_copy(at, f_send.at[columns + i], sib).start()
+        return carry
+
+    lax.fori_loop(1, columns, forward, 0)
+
+    def forward_beside(i, carry):
+        at = source(i, 1 - side)
+        gather_copy(at, f_send.at[2 * columns + i], sib).wait_recv()
+        gather_copy(at, f_send.at[2 * columns + i], sib).start()
+        return carry
+
+    lax.fori_loop(0, columns, forward_beside, 0)
 
     for i in range(8, 12):
         loads[i].wait()
@@ -350,7 +385,7 @@
 
     def arrived(i, carry):
         at = (1 - core) * chips + i
-        gather_copy(at, g_send.at[0], sib).wait_recv()
+        gather_copy(at, f_send.at[0], sib).wait_recv()
         return carry
 
     lax.fori_loop(0, chips, arrived, 0)
@@ -406,13 +441,13 @@
         gather_copy(slot, g_send.at[i], sib).wait_send()
         return carry
 
-    lax.fori_loop(0, chips, drain_gather, 0)
+    lax.fori_loop(1, columns, drain_gather, 0)
 
     def drain_forward(i, carry):
         gather_copy(slot, f_send.at[i], sib).wait_send()
         return carry
 
-    lax.fori_loop(1, chips, drain_forward, 0)
+    lax.fori_loop(0, 3 * columns, drain_forward, 0)
 
     def drain_result(i, carry):
         to = lax.rem(me + i, n_all)
@@ -490,14 +525,14 @@
         dma((12,)),
         dma((6, n_tp)),
         dma((6, n_tp)),
-        dma((chips,)),
-        dma((chips,)),
+        dma((chips // 2,)),
+        dma((3 * (chips // 2),)),
         dma((n_ep,)),
         dma((2,)),
         dma((n_all,)),
         dma((n_all,)),
     ]
-    return pl.pallas_call(
+    outs = pl.pallas_call(
         functools.partial(layer_kernel, n_ep, n_tp),
         out_shape=(
             jax.ShapeDtypeStruct((rows, half), BF16),
@@ -520,8 +555,8 @@
         sub_gain.reshape(1, -1),
         norm_gain_mix.reshape(1, -1),
         branch_gate.reshape(1, -1),
-        route_ids,
-        route_logits,
+        route_ids.T,
+        route_logits.T,
         query_weight,
         key_weight,
         value_weight,
@@ -535,6 +570,12 @@
         dense_up,
         dense_down,
     )
+    return pl.pallas_call(
+        hand_on,
+        out_shape=tuple(jax.ShapeDtypeStruct(o.shape, o.dtype) for o in outs),
+        in_specs=[vmem] * 3,
+        out_specs=(vmem, vmem, vmem),
+    )(*outs)
 
 
 def solution(mesh):

time: 45.4 us -> 42.3 us (0.932)
  local copies, waits for them, and re-layouts: 6.64 us -> 0 us
  Pallas kernels: 37.6 us -> 41.5 us
    unnamed x5 -> x0, local copies, waits for them, and re-layouts: 6.64 us -> none
    pallas_call x1, Pallas kernels: 37.6 us -> 40.1 us  [body(): pl.pallas_call(functools.partial(layer_kernel, n_ep, n_tp), out_shape=(ja...]
    pallas_call x0 -> x1, Pallas kernels: none -> 1.35 us  [body(): pl.pallas_call(hand_on, out_shape=tuple((jax.ShapeDtypeStruct(o.shape, o....]
where the time goes in v2:
time: 42.3 us; the launch traced here: 42.1 us
  Pallas kernels  41.5 us (98%)
  between operations  0.65 us (2%)
    pallas_call x1, Pallas kernels, body(): pl.pallas_call(functools.partial(layer_kernel, n_ep, n_tp), out_shape=(ja...  40.1 us
    pallas_call x1, Pallas kernels, body(): pl.pallas_call(hand_on, out_shape=tuple((jax.ShapeDtypeStruct(o.shape, o....  1.35 us

profile of v2, /device:TPU:0, one launch (start us, length us, event | category | flops | bytes accessed | tf_op | source)
XLA Modules:
  0.0 42.1 jit_solution(9373196634512151166)
XLA Ops:
  0.6 40.1 %shard_map.238 = (bf16[16,512]{1,0:T(8,128)(2,1)}, bf16[16,256]{1,0:T(8,128)(2,1)}, bf16[16,256]{1,0:T(8,128)(2,1)}) custom-call(f32[2]{0:T(128)} %lam_ref.1, s32[16]{0:T(128)} %len_ref.1, bf16[16,512]{1,0:T(8,128)(2,1)} %hid_ref.1, f32[1,1024]{1,0:T(1,128)} %bitcast.8, f32[1,128]{1,0:T(1,128)} %bitcast.13, f32[1,128]{1,0:T(1,128)} %bitcast.14, ...), custom_call_target="tpu_custom_call" | custom-call | tf_op jit(solution)/shard_map/pallas_call | solution.py:535
  40.8 1.4 %shard_map.239 = (bf16[16,512]{1,0:T(8,128)(2,1)}, bf16[16,256]{1,0:T(8,128)(2,1)}, bf16[16,256]{1,0:T(8,128)(2,1)}) custom-call(bf16[16,512]{1,0:T(8,128)(2,1)} %get-tuple-element.6.a_ref, bf16[16,256]{1,0:T(8,128)(2,1)} %get-tuple-element.7.b_ref, bf16[16,256]{1,0:T(8,128)(2,1)} %get-tuple-element.8.c_ref), custom_call_target="tpu_custom_call" | custom-call | tf_op jit(solution)/shard_map/pallas_call | solution.py:573
